TPU v7x, 32 devices: a whole 2x2x4 slice. The times are simulated.
32 devices in a mesh: ep: 16 (over z, y, x), tp: 2 (over core).
Axes of the slice: x: 2, y: 2, z: 4, core: 2. Of those that a mesh axis runs over, the one named last changes fastest.
Arguments:
- inputs: bfloat16 [8192, 2048], P(('ep', 'tp')), may hold values from -6 to 6
- pre_gain: float32 [2048], replicated, may hold values from 0.5 to 8
- expert_ids: int32 [8192, 2], P(('ep', 'tp')), may hold values from 0 to 15, all different within a row; in each aligned block of 256 rows (0 to 255, 256 to 511, ...) at most 48 rows name the same one
- route_weights: float32 [8192, 2], P(('ep', 'tp')), may hold values from 0.05 to 1
- gate_proj: bfloat16 [16, 2048, 2048], P('ep', None, 'tp'), may hold values from -0.125 to 0.125
- up_proj: bfloat16 [16, 2048, 2048], P('ep', None, 'tp'), may hold values from -0.125 to 0.125
- down_proj: bfloat16 [16, 2048, 2048], P('ep', 'tp'), may hold values from -0.125 to 0.125
- post_gain: float32 [2048], replicated, may hold values from 0.1 to 1.9
Outputs:
- layer_out: bfloat16 [8192, 2048], P(('ep', 'tp'))
Inputs may be any that keep to these rules, and one draw needn't show every extreme that they name: `expert_ids`: each token names 2 different experts. Among the 256 tokens of one device (aligned blocks of rows) no expert is named by more than 48 tokens, and in every draw some expert is named by exactly 48 tokens of some device.
All inputs are finite; a program needn't handle non-finite values.
Results may differ from a plain program's by a relative error of at most 0.0095.
Values may be sent and summed in bfloat16 or wider, within the bound.
A program may use at most 128 MiB of HBM per device.

v0:
```python
import jax
import jax.numpy as jnp
from jax import lax
from jax.sharding import PartitionSpec as P

EPSILON = 1e-06
LIMIT = 7.0
ALPHA = 1.702


def norm_rows(values, gain):
    floats = values.astype(jnp.float32)
    return floats * lax.rsqrt(jnp.mean(floats * floats, axis=-1, keepdims=True) + EPSILON) * gain


def activate(gate, up):
    gate = jnp.minimum(gate, LIMIT)
    up = jnp.clip(up, -LIMIT, LIMIT)
    return ((up + 1.0) * gate * jax.nn.sigmoid(ALPHA * gate)).astype(jnp.bfloat16)


def expand(rows, w_gate, w_up):
    gate = jnp.einsum("secd,edf->secf", rows, w_gate, preferred_element_type=jnp.float32)
    up = jnp.einsum("secd,edf->secf", rows, w_up, preferred_element_type=jnp.float32)
    return activate(gate, up)


def local(inputs, pre_gain, expert_ids, route_weights, gate_proj, up_proj, down_proj, post_gain):
    token_count, width = inputs.shape
    choose_count = expert_ids.shape[1]
    ep_count = lax.axis_size("ep")
    tp_count = lax.axis_size("tp")
    local_experts = gate_proj.shape[0]
    experts = local_experts * ep_count
    capacity = 3 * token_count * choose_count // (2 * experts)
    normed = norm_rows(inputs, pre_gain).astype(jnp.bfloat16)
    flat_ids = expert_ids.reshape(-1)
    one_hot = (flat_ids[:, None] == jnp.arange(experts, dtype=jnp.int32)[None, :]).astype(jnp.int32)
    earlier = jnp.cumsum(one_hot, axis=0) - one_hot
    slot = jnp.sum(earlier * one_hot, axis=1)
    target = flat_ids * capacity + slot
    copies = jnp.repeat(normed, choose_count, axis=0)
    buffer = jnp.zeros((experts * capacity, width), jnp.bfloat16).at[target].set(copies)
    buffer = buffer.reshape(experts, capacity, width)
    gate_full, up_full = (
        lax.all_gather(gate_proj, "tp", axis=2, tiled=True),
        lax.all_gather(up_proj, "tp", axis=2, tiled=True),
    )
    down_full = lax.all_gather(down_proj, "tp", axis=1, tiled=True)
    received = lax.all_to_all(buffer, "ep", split_axis=0, concat_axis=0, tiled=True)
    count = received.shape[1]
    rows = received.reshape(ep_count, local_experts, count, width)
    half = down_proj.shape[1]
    total = jnp.zeros((ep_count, local_experts, count, width), jnp.float32)
    for index in range(tp_count):
        lower = index * half
        hidden = expand(
            rows, gate_full[:, :, lower : lower + half], up_full[:, :, lower : lower + half]
        )
        part = jnp.einsum(
            "secf,efd->secd",
            hidden,
            down_full[:, lower : lower + half],
            preferred_element_type=jnp.float32,
        )
        part = lax.optimization_barrier(part.astype(jnp.bfloat16))
        total = total + part.astype(jnp.float32)
    result = total.astype(jnp.bfloat16)
    returned = lax.all_to_all(
        result.reshape(ep_count * local_experts, count, width),
        "ep",
        split_axis=0,
        concat_axis=0,
        tiled=True,
    )
    picked = returned.reshape(experts * capacity, width)[target]
    picked = picked.reshape(token_count, choose_count, width).astype(jnp.float32)
    mixed = jnp.sum(picked * route_weights[:, :, None], axis=1)
    return norm_rows(mixed, post_gain).astype(jnp.bfloat16)


def solution(mesh):
    in_specs = (
        P(("ep", "tp"), None),
        P(),
        P(("ep", "tp"), None),
        P(("ep", "tp"), None),
        P("ep", None, "tp"),
        P("ep", None, "tp"),
        P("ep", "tp", None),
        P(),
    )
    out_specs = P(("ep", "tp"), None)
    return jax.shard_map(local, mesh=mesh, in_specs=in_specs, out_specs=out_specs, check_vma=False)
```

profile of v0, /device:TPU:12, one launch (start us, length us, event | category | flops | bytes accessed | tf_op | source)
XLA Modules:
  0.0 247.9 jit_solution(10718546624715610538)
XLA Ops:
  6.5 0.0 all-gather.6.cloned.1.call-start
  6.5 0.7 all-gather.6.cloned.1.call-update
  7.3 0.0 all-gather.4.cloned.1.call-start
  7.3 0.7 all-gather.4.cloned.1.call-update
  8.0 0.0 copy-start.4
  8.0 0.0 copy-start
  8.0 0.0 copy-start.2
  8.0 0.0 all-gather.8.cloned.1.call-start
  8.1 0.7 all-gather.8.cloned.1.call-update
  8.8 0.0 copy-done.4
  8.8 0.1 copy.11
  8.9 0.1 eq.29
  9.1 0.1 eq.25
  9.2 1.2 reduce-window.6
  10.4 0.2 slice_reduce_fusion
  10.6 0.1 copy.10
  10.8 0.1 mul.105
  10.9 0.0 copy-done
  10.9 0.3 fusion.11
  11.2 0.0 copy-done.2
  11.3 0.3 fusion.13
  11.6 1.3 broadcast_in_dim.5
  12.8 2.3 reshape.179
  15.1 0.1 fusion.18
  15.2 6.0 %scatter_custom_fusion = bf16[768,2048]{1,0:T(8,128)(2,1)S(1)} fusion(s32[512]{0:T(512)S(1)} %bitcast.83, bf16[512,2048]{1,0:T(8,128)(2,1)} %reshape.179, bf16[]{:T(256)} %constant.12.clone.1), kind=kCustom, calls=%fused_computation.30 | custom fusion | bytes 3146240 | tf_op jit(solution)/shard_map/scatter | solution.py:43
  21.2 77.2 %all_to_all.10 = bf16[16,48,2048]{2,1,0:T(8,128)(2,1)} all-to-all(bf16[16,48,2048]{2,1,0:T(8,128)(2,1)S(1)} %bitcast.82), channel_id=1, replica_groups=mesh['ep'=16,'tp'=2] {'ep'}, dimensions={0} | all-to-all | bytes 6291456 | tf_op jit(solution)/shard_map/all_to_all | solution.py:50
  98.4 0.0 copy-start.1
  98.4 0.0 all-gather.6.cloned.1.call-done
  98.4 8.4 %fusion.4 = f32[16,48,1024]{2,1,0:T(8,128)} fusion(bf16[16,48,2048]{2,1,0:T(8,128)(2,1)} %all_to_all.10, bf16[1,2048,2048]{2,1,0:T(8,128)(2,1)} %all-gather.6.cloned.1.call-done), kind=kOutput, calls=%fused_computation.12 | convolution fusion | flops 3221225472 | bytes 10485760 | tf_op jit(solution)/shard_map/secd,edf->secf/dot_general | solution.py:23
  106.8 0.0 all-gather.4.cloned.1.call-done
  106.8 0.0 all-gather.8.cloned.1.call-done
  106.8 0.0 copy-done.1
  106.8 13.4 %fusion.10 = bf16[16,1,48,2048]{3,2,0,1:T(8,128)(2,1)} fusion(bf16[1,2048,2048]{2,1,0:T(8,128)(2,1)} %all-gather.8.cloned.1.call-done, f32[16,48,1024]{2,1,0:T(8,128)} %fusion.4, bf16[16,48,2048]{2,1,0:T(8,128)(2,1)S(1)} %copy-done.1, bf16[1,2048,2048]{2,1,0:T(8,128)(2,1)} %all-gather.4.cloned.1.call-done), kind=kOutput, calls=%fused_computation.22 | convolution fusion | flops 6451888128 | bytes 17825792 | tf_op jit(solution)/shard_map/secf,efd->secd/dot_general | solution.py:60
  120.2 7.3 %fusion.1 = f32[16,48,1024]{2,1,0:T(8,128)} fusion(bf16[16,48,2048]{2,1,0:T(8,128)(2,1)S(1)} %copy-done.1, bf16[1,2048,2048]{2,1,0:T(8,128)(2,1)} %all-gather.6.cloned.1.call-done), kind=kOutput, calls=%fused_computation.6 | convolution fusion | flops 3221225472 | bytes 10485760 | tf_op jit(solution)/shard_map/secd,edf->secf/dot_general | solution.py:23
  127.5 13.5 %fusion.9 = bf16[16,1,48,2048]{3,2,0,1:T(8,128)(2,1)} fusion(bf16[1,2048,2048]{2,1,0:T(8,128)(2,1)} %all-gather.8.cloned.1.call-done, f32[16,48,1024]{2,1,0:T(8,128)} %fusion.1, bf16[16,48,2048]{2,1,0:T(8,128)(2,1)S(1)} %copy-done.1, bf16[1,2048,2048]{2,1,0:T(8,128)(2,1)} %all-gather.4.cloned.1.call-done), kind=kOutput, calls=%fused_computation.21 | convolution fusion | flops 6451888128 | bytes 17825792 | tf_op jit(solution)/shard_map/secf,efd->secd/dot_general | solution.py:60
  141.1 6.1 %fusion.8 = bf16[16,48,2048]{2,1,0:T(8,128)(2,1)} fusion(bf16[16,1,48,2048]{3,2,0,1:T(8,128)(2,1)} %fusion.9, bf16[16,1,48,2048]{3,2,0,1:T(8,128)(2,1)} %fusion.10), kind=kLoop, calls=%fused_computation.18 | loop fusion | flops 6291456 | bytes 9437184 | tf_op jit(solution)/shard_map/reshape | solution.py:70
  147.2 0.0 copy-start.5
  147.2 5.2 %all-to-all-start.1 = ((bf16[16,48,2048]{2,1,0:T(8,128)(2,1)}), bf16[16,48,2048]{2,1,0:T(8,128)(2,1)S(1)}, u32[]{:S(2)}, u32[]{:S(2)}) async-start(bf16[16,48,2048]{2,1,0:T(8,128)(2,1)} %fusion.8), calls=%async_computation.1 | async-start | bytes 6291456 | tf_op jit(solution)/shard_map/all_to_all | solution.py:69
  152.4 0.0 copy-done.5
  152.4 0.1 copy.14
  152.6 69.8 %all-to-all-done.1 = bf16[16,48,2048]{2,1,0:T(8,128)(2,1)S(1)} async-done(((bf16[16,48,2048]{2,1,0:T(8,128)(2,1)}), bf16[16,48,2048]{2,1,0:T(8,128)(2,1)S(1)}, u32[]{:S(2)}, u32[]{:S(2)}) %all-to-all-start.1) | async-done | bytes 3145760 | tf_op jit(solution)/shard_map/all_to_all | solution.py:69
  222.3 3.3 %gather_fusion = bf16[512,2048]{1,0:T(8,128)(2,1)} fusion(bf16[768,2048]{1,0:T(8,128)(2,1)S(1)} %bitcast.81, s32[1024]{0:T(1024)S(1)} %pad_clamp_fusion), kind=kCustom, calls=%fused_computation | custom fusion | bytes 4196352 | tf_op jit(solution)/shard_map/gather | solution.py:76
  225.6 5.4 %reshape.156 = f32[256,2,2048]{2,1,0:T(2,128)} reshape(bf16[512,2048]{1,0:T(8,128)(2,1)} %gather_fusion) | data formatting | bytes 6291456 | tf_op jit(solution)/shard_map/convert_element_type | solution.py:77
  231.1 0.0 copy-start.3
  231.1 8.9 %multiply_reduce_fusion = f32[256,2048]{1,0:T(8,128)S(1)} fusion(f32[256,2,2048]{2,1,0:T(2,128)} %reshape.156, f32[256,2]{1,0:T(8,128)S(1)} %copy.14), kind=kLoop, calls=%fused_computation.15 | loop fusion | flops 1572864 | bytes 6293504 | tf_op jit(solution)/shard_map/reduce_sum | solution.py:78
  240.0 0.2 multiply_reduce_fusion.1
  240.2 0.0 copy-done.3
  240.2 1.2 multiply_convert_fusion.2
  (8 shorter events, 0.1 us)
Async XLA Ops:
  6.5 91.9 %all-gather.6.cloned.1.call-start = ((), (), s32[]{:S(2)}) async-start(), calls=%async_computation.3 | async-start | bytes 12582912 | tf_op jit(solution)/shard_map/all_gather | solution.py:46
  7.3 99.6 %all-gather.4.cloned.1.call-start = ((), (), s32[]{:S(2)}) async-start(), calls=%async_computation.2 | async-start | bytes 12582912 | tf_op jit(solution)/shard_map/all_gather | solution.py:47
  8.0 0.8 copy-start.4
  8.0 2.9 %copy-start = (bf16[256,2048]{1,0:T(8,128)(2,1)S(1)}, bf16[256,2048]{1,0:T(8,128)(2,1)}, u32[]{:S(2)}) copy-start(bf16[256,2048]{1,0:T(8,128)(2,1)} %param.8) | copy-start | bytes 3145732
  8.0 3.2 %copy-start.2 = (f32[2048]{0:T(1024)S(1)}, f32[2048]{0:T(1024)}, u32[]{:S(2)}) copy-start(f32[2048]{0:T(1024)} %param.9) | copy-start | bytes 24580
  8.0 98.8 %all-gather.8.cloned.1.call-start = ((), (), s32[]{:S(2)}) async-start(), calls=%async_computation.4 | async-start | bytes 12582912 | tf_op jit(solution)/shard_map/all_gather | solution.py:49
  98.4 8.5 %copy-start.1 = (bf16[16,48,2048]{2,1,0:T(8,128)(2,1)S(1)}, bf16[16,48,2048]{2,1,0:T(8,128)(2,1)}, u32[]{:S(2)}) copy-start(bf16[16,48,2048]{2,1,0:T(8,128)(2,1)} %all_to_all.10) | copy-start | bytes 9437188
  147.2 5.2 %copy-start.5 = (f32[256,2]{0,1:T(2,128)S(1)}, f32[256,2]{0,1:T(2,128)}, u32[]{:S(2)}) copy-start(f32[256,2]{0,1:T(2,128)} %param.11) | copy-start | bytes 6148
  147.2 75.1 %all-to-all-start.1 = ((bf16[16,48,2048]{2,1,0:T(8,128)(2,1)}), bf16[16,48,2048]{2,1,0:T(8,128)(2,1)S(1)}, u32[]{:S(2)}, u32[]{:S(2)}) async-start(bf16[16,48,2048]{2,1,0:T(8,128)(2,1)} %fusion.8), calls=%async_computation.1 | async-start | bytes 6291456 | tf_op jit(solution)/shard_map/all_to_all | solution.py:69
  231.1 9.1 %copy-start.3 = (f32[2048]{0:T(1024)S(1)}, f32[2048]{0:T(1024)}, u32[]{:S(2)}) copy-start(f32[2048]{0:T(1024)} %param.15) | copy-start | bytes 24580
Sparse Core Ops, SparseCore 0:
  8.9 21.2 all-gather.5
  31.7 21.0 all-gather.3
  54.3 21.0 all-gather.7
where the time goes:
time: 248 us
  blocking collectives  77.2 us (31%)
  waiting for transfers between devices  71.8 us (29%)
  matrix products  42.7 us (17%)
  local copies, waits for them, and re-layouts  19.4 us (8%)
  other arithmetic  18.3 us (7%)
  between operations  13.3 us (5%)
  starting transfers between devices  5.3 us (2%)
    all_to_all x1, blocking collectives, local(): lax.all_to_all(buffer, 'ep', split_axis=0, concat_axis=0, tiled=True)  77.2 us
    all_to_all x1, waiting for transfers between devices, local(): lax.all_to_all(result.reshape(ep_count * local_experts, count, width), 'e...  69.8 us
    dot_general x2, matrix products, local(): jnp.einsum('secf,efd->secd', hidden, down_full[:, lower:lower + half], pr...  26.9 us
    dot_general x2, matrix products, expand(): jnp.einsum('secd,edf->secf', rows, w_gate, preferred_element_type=jnp.flo...  15.8 us
    reduce_sum x1, other arithmetic, local(): mixed = jnp.sum(picked * route_weights[:, :, None], axis=1)  8.89 us
    reshape x1, other arithmetic, local(): result.reshape(ep_count * local_experts, count, width)  6.09 us
    scatter x1, local copies, waits for them, and re-layouts, local(): jnp.zeros((experts * capacity, width), jnp.bfloat16).at[target].set(copies)  5.98 us
    convert_element_type x1, local copies, waits for them, and re-layouts, local(): picked.reshape(token_count, choose_count, width).astype(jnp.float32)  5.44 us
  transfers between devices with their start and end apart: 4, of which 1 were waited for; matrix products, arithmetic and copies ran while one was open for 8% of the time, Pallas kernels for 0%

commit v1 on v0

v1 whole, which is shorter than its diff:
```python
import functools

import jax
import jax.numpy as jnp
from jax import lax
from jax.experimental import pallas as pl
from jax.experimental.pallas import tpu as pltpu
from jax.sharding import PartitionSpec as P

EPSILON = 1e-06
LIMIT = 7.0
ALPHA = 1.702
CHUNKS = 4
TILE = 256
MESH = pl.DeviceIdType.MESH


def activate(gate, up):
    gate = jnp.minimum(gate, LIMIT)
    up = jnp.clip(up, -LIMIT, LIMIT)
    return ((up + 1.0) * gate * jax.nn.sigmoid(ALPHA * gate)).astype(jnp.bfloat16)


def dot(a, b):
    return jnp.dot(a, b, preferred_element_type=jnp.float32)


def kernel(
    n, tps, cap,
    x_ref, pre_ref, meta_ref, gate_ref, up_ref, down_ref, post_ref, out_ref,
    gate_v, up_v, down_v, normed, prox, pmeta, send, recv, res, ret, part_send, part_recv,
    mixed, hidden, places,
    w_local, w_send, w_recv, p_send, p_recv, m_send, m_recv,
    d_send, d_recv, r_send, r_recv, q_send, q_recv,
):
    half = n // 2
    tokens, width = x_ref.shape
    cw = width // CHUNKS
    rows = half * cap
    fh = gate_v.shape[2]
    me = lax.axis_index("ep")
    core = lax.axis_index("tp")
    base = (me // half) * half
    mine = lax.rem(me, half)
    proxy = lax.rem(me + half, n)

    def member(j):
        return base + lax.rem(mine + j, half)

    barrier = pltpu.get_barrier_semaphore()

    @pl.loop(1, half)
    def _(j):
        pl.semaphore_signal(barrier, inc=1, device_id={"ep": member(j)}, device_id_type=MESH)

    pl.semaphore_signal(barrier, inc=1, device_id={"ep": proxy}, device_id_type=MESH)
    for i in range(1, tps):
        pl.semaphore_signal(
            barrier, inc=1, device_id={"tp": lax.rem(core + i, tps)}, device_id_type=MESH
        )
    pl.semaphore_wait(barrier, half + tps - 1)

    def remote(src, dst, ss, rs, where):
        return pltpu.make_async_remote_copy(
            src_ref=src, dst_ref=dst, send_sem=ss, recv_sem=rs,
            device_id=where, device_id_type=MESH,
        )

    def await_bytes(ref, sem):
        pltpu.make_async_copy(ref, ref, sem).wait()

    remote(meta_ref, pmeta, m_send, m_recv, {"ep": proxy}).start()
    weights = ((gate_ref, gate_v), (up_ref, up_v), (down_ref, down_v))
    local_copies, peer_copies = [], []
    for w, (src, dst) in enumerate(weights):
        local_copies.append(pltpu.make_async_copy(src.at[0], dst.at[core], w_local.at[w]))
        for i in range(1, tps):
            peer_copies.append(
                remote(
                    src.at[0], dst.at[core], w_send.at[w, i - 1], w_recv.at[w, i - 1],
                    {"tp": lax.rem(core + i, tps)},
                )
            )
    for copy in peer_copies + local_copies:
        copy.start()

    experts_col = lax.broadcasted_iota(jnp.int32, (n, 1), 0).astype(jnp.float32)
    earlier_mask = (
        lax.broadcasted_iota(jnp.int32, (tokens, tokens), 0)
        < lax.broadcasted_iota(jnp.int32, (tokens, tokens), 1)
    ).astype(jnp.bfloat16)

    def place(k, meta):
        first, second = meta[0:1, :], meta[1:2, :]
        hot0 = (first == experts_col).astype(jnp.float32)
        hot1 = (second == experts_col).astype(jnp.float32)
        before = dot((hot0 + hot1).astype(jnp.bfloat16), earlier_mask)
        places[k] = meta
        for i, (ids, hot) in enumerate(((first, hot0), (second, hot1))):
            slot = jnp.sum(before * hot, axis=0, keepdims=True)
            relative = ids - (base + mine).astype(jnp.float32)
            inside = (ids >= base.astype(jnp.float32)) & (
                ids < (base + half).astype(jnp.float32)
            )
            relative = jnp.where(relative < 0, relative + half, relative)
            places[k, i : i + 1, :] = jnp.where(inside, relative * cap + slot, -1.0)

    def picker(k):
        at = lax.broadcasted_iota(jnp.int32, (rows, 1), 0).astype(jnp.float32)
        return (
            (places[k, 0:1, :] == at).astype(jnp.float32)
            + (places[k, 1:2, :] == at).astype(jnp.float32)
        ).astype(jnp.bfloat16)

    def mixer(k):
        columns = places[k].T
        at = lax.broadcasted_iota(jnp.int32, (1, rows), 1).astype(jnp.float32)
        w = jnp.where(columns[:, 0:1] == at, columns[:, 2:3], 0.0) + jnp.where(
            columns[:, 1:2] == at, columns[:, 3:4], 0.0
        )
        high = w.astype(jnp.bfloat16)
        return high, (w - high.astype(jnp.float32)).astype(jnp.bfloat16)

    def dispatch(k, c, values):
        picked = dot(picker(k), values).astype(jnp.bfloat16)
        recv[k, c, 0:cap, :] = picked[0:cap]
        send[k, c, cap:rows, :] = picked[cap:rows]

        @pl.loop(1, half)
        def _(j):
            block = pl.ds(pl.multiple_of(j * cap, cap), cap)
            remote(
                send.at[k, c, block], recv.at[k, c, block], d_send.at[k, c], d_recv.at[k, c],
                {"ep": member(j)},
            ).start()

    def give_back(k, c):
        @pl.loop(1, half)
        def _(j):
            block = pl.ds(pl.multiple_of(j * cap, cap), cap)
            remote(
                res.at[k, c, block], ret.at[k, c, block], r_send.at[k, c], r_recv.at[k, c],
                {"ep": member(half - j)},
            ).start()

    place(0, meta_ref[...])
    squares = jnp.zeros((tokens, 1), jnp.float32)
    for c in range(CHUNKS):
        xs = x_ref[:, c * cw : (c + 1) * cw].astype(jnp.float32)
        squares = squares + jnp.sum(xs * xs, axis=-1, keepdims=True)
    scale = lax.rsqrt(squares / width + EPSILON)
    proxied = []
    for c in range(CHUNKS):
        xs = x_ref[:, c * cw : (c + 1) * cw].astype(jnp.float32)
        normed[c] = (xs * scale * pre_ref[:, c * cw : (c + 1) * cw]).astype(jnp.bfloat16)
        copy = remote(normed.at[c], prox.at[c], p_send.at[c], p_recv.at[c], {"ep": proxy})
        copy.start()
        proxied.append(copy)
        dispatch(0, c, normed[c])

    meta_copy = remote(meta_ref, pmeta, m_send, m_recv, {"ep": proxy})
    meta_copy.wait_recv()
    place(1, pmeta[...])

    def relay(c):
        proxied[c].wait_recv()
        dispatch(1, c, prox[c])

    def received(k):
        for c in range(CHUNKS):
            await_bytes(recv.at[k, c, pl.ds(cap, rows - cap)], d_recv.at[k, c])

    def expand(k):
        for h in range(tps):
            @pl.loop(0, fh // TILE)
            def _(t):
                at = pl.ds(pl.multiple_of(t * TILE, TILE), TILE)
                gate = jnp.zeros((rows, TILE), jnp.float32)
                up = jnp.zeros((rows, TILE), jnp.float32)
                for c in range(CHUNKS):
                    gate += dot(recv[k, c], gate_v[h, c * cw : (c + 1) * cw, at])
                    up += dot(recv[k, c], up_v[h, c * cw : (c + 1) * cw, at])
                hidden[h, :, at] = activate(gate, up)

    def contract(k, c):
        for t in range(cw // TILE):
            lo = t * TILE
            total = jnp.zeros((rows, TILE), jnp.float32)
            for h in range(tps):
                at = pl.ds(pl.multiple_of(c * cw + lo, TILE), TILE)
                total += dot(hidden[h], down_v[h, :, at]).astype(jnp.bfloat16).astype(jnp.float32)
            total = total.astype(jnp.bfloat16)
            ret[k, c, 0:cap, lo : lo + TILE] = total[0:cap]
            res[k, c, cap:rows, lo : lo + TILE] = total[cap:rows]
        give_back(k, c)

    relay(0)
    relay(1)
    for copy in local_copies:
        copy.wait()
    for copy in peer_copies:
        copy.wait()
    received(0)
    expand(0)
    relay(2)

    @pl.loop(0, CHUNKS)
    def _(c):
        contract(0, c)

    relay(3)
    received(1)
    expand(1)

    @pl.loop(0, CHUNKS)
    def _(c):
        contract(1, c)

    high0, low0 = mixer(0)
    for c in range(CHUNKS):
        await_bytes(ret.at[0, c, pl.ds(cap, rows - cap)], r_recv.at[0, c])
        mixed[c] = dot(high0, ret[0, c]) + dot(low0, ret[0, c])
    high1, low1 = mixer(1)
    shares = []
    for c in range(CHUNKS):
        await_bytes(ret.at[1, c, pl.ds(cap, rows - cap)], r_recv.at[1, c])
        part_send[c] = (dot(high1, ret[1, c]) + dot(low1, ret[1, c])).astype(jnp.bfloat16)
        copy = remote(part_send.at[c], part_recv.at[c], q_send.at[c], q_recv.at[c], {"ep": proxy})
        copy.start()
        shares.append(copy)

    squares = jnp.zeros((tokens, 1), jnp.float32)
    for c in range(CHUNKS):
        shares[c].wait_recv()
        total = mixed[c] + part_recv[c].astype(jnp.float32)
        mixed[c] = total
        squares = squares + jnp.sum(total * total, axis=-1, keepdims=True)
    scale = lax.rsqrt(squares / width + EPSILON)
    for c in range(CHUNKS):
        at = slice(c * cw, (c + 1) * cw)
        out_ref[:, at] = (mixed[c] * scale * post_ref[:, at]).astype(jnp.bfloat16)

    meta_copy.wait_send()
    for c in range(CHUNKS):
        proxied[c].wait_send()
        shares[c].wait_send()
        for k in range(2):
            await_bytes(send.at[k, c, pl.ds(cap, rows - cap)], d_send.at[k, c])
            await_bytes(res.at[k, c, pl.ds(cap, rows - cap)], r_send.at[k, c])


def local(inputs, pre_gain, expert_ids, route_weights, gate_proj, up_proj, down_proj, post_gain):
    tokens, width = inputs.shape
    choices = expert_ids.shape[1]
    n = lax.axis_size("ep")
    tps = lax.axis_size("tp")
    cap = 3 * tokens * choices // (2 * n * gate_proj.shape[0])
    cap = -(-cap // 16) * 16
    half = n // 2
    rows = half * cap
    cw = width // CHUNKS
    fh = gate_proj.shape[2]
    meta = jnp.concatenate(
        [
            expert_ids.astype(jnp.float32),
            route_weights,
            jnp.zeros((tokens, 8 - 2 * choices), jnp.float32),
        ],
        axis=1,
    ).T
    bf16 = jnp.bfloat16
    vmem = pl.BlockSpec(memory_space=pltpu.VMEM)
    hbm = pl.BlockSpec(memory_space=pl.ANY)
    dma = pltpu.SemaphoreType.DMA
    return pl.pallas_call(
        functools.partial(kernel, n, tps, cap),
        out_shape=jax.ShapeDtypeStruct((tokens, width), bf16),
        in_specs=[vmem, vmem, vmem, hbm, hbm, hbm, vmem],
        out_specs=vmem,
        scratch_shapes=[
            pltpu.VMEM((tps, width, fh), bf16),
            pltpu.VMEM((tps, width, fh), bf16),
            pltpu.VMEM((tps, fh, width), bf16),
            pltpu.VMEM((CHUNKS, tokens, cw), bf16),
            pltpu.VMEM((CHUNKS, tokens, cw), bf16),
            pltpu.VMEM((8, tokens), jnp.float32),
            pltpu.VMEM((2, CHUNKS, rows, cw), bf16),
            pltpu.VMEM((2, CHUNKS, rows, cw), bf16),
            pltpu.VMEM((2, CHUNKS, rows, cw), bf16),
            pltpu.VMEM((2, CHUNKS, rows, cw), bf16),
            pltpu.VMEM((CHUNKS, tokens, cw), bf16),
            pltpu.VMEM((CHUNKS, tokens, cw), bf16),
            pltpu.VMEM((CHUNKS, tokens, cw), jnp.float32),
            pltpu.VMEM((tps, rows, fh), bf16),
            pltpu.VMEM((2, 8, tokens), jnp.float32),
            dma((3,)), dma((3, tps - 1)), dma((3, tps - 1)),
            dma((CHUNKS,)), dma((CHUNKS,)), dma, dma,
            dma((2, CHUNKS)), dma((2, CHUNKS)), dma((2, CHUNKS)), dma((2, CHUNKS)),
            dma((CHUNKS,)), dma((CHUNKS,)),
        ],
        compiler_params=pltpu.CompilerParams(
            collective_id=0, has_side_effects=True, vmem_limit_bytes=67043328
        ),
    )(inputs, pre_gain[None, :], meta, gate_proj, up_proj, down_proj, post_gain[None, :])


def solution(mesh):
    in_specs = (
        P(("ep", "tp"), None),
        P(),
        P(("ep", "tp"), None),
        P(("ep", "tp"), None),
        P("ep", None, "tp"),
        P("ep", None, "tp"),
        P("ep", "tp", None),
        P(),
    )
    out_specs = P(("ep", "tp"), None)
    return jax.shard_map(local, mesh=mesh, in_specs=in_specs, out_specs=out_specs, check_vma=False)
```

time: 248 us -> 151 us (0.61)
  the two profiles are of different devices: /device:TPU:12 before, /device:TPU:0 now
where the time goes in v1:
time: 151 us
  Pallas kernels  147 us (97%)
  local copies, waits for them, and re-layouts  2.38 us (2%)
  other arithmetic  2.03 us (1%)
    pallas_call x1, Pallas kernels, local(): pl.pallas_call(functools.partial(kernel, n, tps, cap), out_shape=jax.Shap...  147 us

profile of v1, /device:TPU:0, one launch (start us, length us, event | category | flops | bytes accessed | tf_op | source)
XLA Modules:
  0.0 151.0 jit_solution(8520433931694203849)
XLA Ops:
  0.0 0.1 pad.2.clone
  0.1 0.7 convert_element_type.3
  0.8 1.3 maximum_bitcast_fusion.meta_ref
  2.1 146.6 %shard_map.82 = bf16[256,2048]{1,0:T(8,128)(2,1)} custom-call(bf16[256,2048]{1,0:T(8,128)(2,1)} %x_ref.1, f32[1,2048]{1,0:T(1,128)} %bitcast.4, f32[8,256]{1,0:T(8,128)} %maximum_bitcast_fusion.meta_ref, bf16[1,2048,1024]{2,1,0:T(8,128)(2,1)} %gate_ref.1, bf16[1,2048,1024]{2,1,0:T(8,128)(2,1)} %up_ref.1, bf16[1,1024,2048]{2,1,0:T(8,128)(2,1)} %down_ref.1, ...), custom_call_target="tpu_custom_call" | custom-call | tf_op jit(solution)/shard_map/pallas_call | solution.py:275
  148.7 2.3 %copy.10 = bf16[256,2048]{1,0:T(8,128)(2,1)} copy(bf16[256,2048]{1,0:T(8,128)(2,1)} %shard_map.82) | data formatting | bytes 2097152
  (1 shorter events, 0.0 us)

commit v2 on v1

--- a/solution.py
+++ b/solution.py
@@ -28,7 +28,7 @@
 def kernel(
     n, tps, cap,
     x_ref, pre_ref, meta_ref, gate_ref, up_ref, down_ref, post_ref, out_ref,
-    gate_v, up_v, down_v, normed, prox, pmeta, send, recv, res, ret, part_send, part_recv,
+    gate_v, up_v, down_v, normed, prox, pmeta, send, recv, ret, acc, part_send, part_recv,
     mixed, hidden, places,
     w_local, w_send, w_recv, p_send, p_recv, m_send, m_recv,
     d_send, d_recv, r_send, r_recv, q_send, q_recv,
@@ -139,96 +139,137 @@
         def _(j):
             block = pl.ds(pl.multiple_of(j * cap, cap), cap)
             remote(
-                res.at[k, c, block], ret.at[k, c, block], r_send.at[k, c], r_recv.at[k, c],
+                send.at[k, c, block], ret.at[k, c, block], r_send.at[k, c], r_recv.at[k, c],
                 {"ep": member(half - j)},
             ).start()
 
-    place(0, meta_ref[...])
     squares = jnp.zeros((tokens, 1), jnp.float32)
     for c in range(CHUNKS):
         xs = x_ref[:, c * cw : (c + 1) * cw].astype(jnp.float32)
         squares = squares + jnp.sum(xs * xs, axis=-1, keepdims=True)
     scale = lax.rsqrt(squares / width + EPSILON)
-    proxied = []
-    for c in range(CHUNKS):
+    proxied = [
+        remote(normed.at[c], prox.at[c], p_send.at[c], p_recv.at[c], {"ep": proxy})
+        for c in range(CHUNKS)
+    ]
+
+    def normalise(c):
         xs = x_ref[:, c * cw : (c + 1) * cw].astype(jnp.float32)
         normed[c] = (xs * scale * pre_ref[:, c * cw : (c + 1) * cw]).astype(jnp.bfloat16)
-        copy = remote(normed.at[c], prox.at[c], p_send.at[c], p_recv.at[c], {"ep": proxy})
-        copy.start()
-        proxied.append(copy)
+
+    def own(c):
         dispatch(0, c, normed[c])
-
-    meta_copy = remote(meta_ref, pmeta, m_send, m_recv, {"ep": proxy})
-    meta_copy.wait_recv()
-    place(1, pmeta[...])
 
     def relay(c):
         proxied[c].wait_recv()
         dispatch(1, c, prox[c])
 
-    def received(k):
-        for c in range(CHUNKS):
-            await_bytes(recv.at[k, c, pl.ds(cap, rows - cap)], d_recv.at[k, c])
-
-    def expand(k):
-        for h in range(tps):
-            @pl.loop(0, fh // TILE)
+    meta_copy = remote(meta_ref, pmeta, m_send, m_recv, {"ep": proxy})
+    normalise(0)
+    proxied[0].start()
+    place(0, meta_ref[...])
+    own(0)
+    normalise(1)
+    proxied[1].start()
+    own(1)
+    normalise(2)
+    normalise(3)
+    meta_copy.wait_recv()
+    place(1, pmeta[...])
+
+    def received(k, c):
+        await_bytes(recv.at[k, c, pl.ds(cap, rows - cap)], d_recv.at[k, c])
+
+    def expand(k, halves, chunks, begin=True, end=True, tiles=(0, fh // TILE)):
+        for h in halves:
+            @pl.loop(*tiles)
             def _(t):
                 at = pl.ds(pl.multiple_of(t * TILE, TILE), TILE)
-                gate = jnp.zeros((rows, TILE), jnp.float32)
-                up = jnp.zeros((rows, TILE), jnp.float32)
-                for c in range(CHUNKS):
+                if begin:
+                    gate = jnp.zeros((rows, TILE), jnp.float32)
+                    up = jnp.zeros((rows, TILE), jnp.float32)
+                else:
+                    gate = acc[0, h, :, at]
+                    up = acc[1, h, :, at]
+                for c in chunks:
                     gate += dot(recv[k, c], gate_v[h, c * cw : (c + 1) * cw, at])
                     up += dot(recv[k, c], up_v[h, c * cw : (c + 1) * cw, at])
-                hidden[h, :, at] = activate(gate, up)
+                if end:
+                    hidden[k, h, :, at] = activate(gate, up)
+                else:
+                    acc[0, h, :, at] = gate
+                    acc[1, h, :, at] = up
 
     def contract(k, c):
+        await_bytes(send.at[k, c, pl.ds(cap, rows - cap)], d_send.at[k, c])
         for t in range(cw // TILE):
             lo = t * TILE
             total = jnp.zeros((rows, TILE), jnp.float32)
             for h in range(tps):
                 at = pl.ds(pl.multiple_of(c * cw + lo, TILE), TILE)
-                total += dot(hidden[h], down_v[h, :, at]).astype(jnp.bfloat16).astype(jnp.float32)
+                total += dot(hidden[k, h], down_v[h, :, at]).astype(jnp.bfloat16).astype(jnp.float32)
             total = total.astype(jnp.bfloat16)
             ret[k, c, 0:cap, lo : lo + TILE] = total[0:cap]
-            res[k, c, cap:rows, lo : lo + TILE] = total[cap:rows]
+            send[k, c, cap:rows, lo : lo + TILE] = total[cap:rows]
         give_back(k, c)
 
+    both = range(tps)
+    last = fh // TILE
     relay(0)
-    relay(1)
+    proxied[2].start()
     for copy in local_copies:
         copy.wait()
     for copy in peer_copies:
         copy.wait()
-    received(0)
-    expand(0)
+    relay(1)
+    proxied[3].start()
+    received(1, 0)
+    received(1, 1)
+    expand(1, both, (0, 1), end=False)
     relay(2)
-
-    @pl.loop(0, CHUNKS)
-    def _(c):
-        contract(0, c)
-
+    received(1, 2)
+    expand(1, both, (2,), begin=False, end=False)
     relay(3)
-    received(1)
-    expand(1)
-
-    @pl.loop(0, CHUNKS)
-    def _(c):
-        contract(1, c)
-
-    high0, low0 = mixer(0)
-    for c in range(CHUNKS):
-        await_bytes(ret.at[0, c, pl.ds(cap, rows - cap)], r_recv.at[0, c])
-        mixed[c] = dot(high0, ret[0, c]) + dot(low0, ret[0, c])
+    own(2)
+    own(3)
+    received(1, 3)
+    expand(1, both, (3,), begin=False)
+
+    shares = []
     high1, low1 = mixer(1)
-    shares = []
-    for c in range(CHUNKS):
+
+    def share(c):
         await_bytes(ret.at[1, c, pl.ds(cap, rows - cap)], r_recv.at[1, c])
         part_send[c] = (dot(high1, ret[1, c]) + dot(low1, ret[1, c])).astype(jnp.bfloat16)
         copy = remote(part_send.at[c], part_recv.at[c], q_send.at[c], q_recv.at[c], {"ep": proxy})
         copy.start()
         shares.append(copy)
 
+    contract(1, 0)
+    contract(1, 1)
+    for c in range(CHUNKS):
+        received(0, c)
+    every = range(CHUNKS)
+    expand(0, (0,), every, tiles=(0, last // 2))
+    share(0)
+    contract(1, 2)
+    expand(0, (0,), every, tiles=(last // 2, last))
+    share(1)
+    contract(1, 3)
+    expand(0, range(1, tps), every, tiles=(0, last // 2))
+    share(2)
+    expand(0, range(1, tps), every, tiles=(last // 2, last))
+    share(3)
+
+    @pl.loop(0, CHUNKS)
+    def _(c):
+        contract(0, c)
+
+    high0, low0 = mixer(0)
+    for c in range(CHUNKS):
+        await_bytes(ret.at[0, c, pl.ds(cap, rows - cap)], r_recv.at[0, c])
+        mixed[c] = dot(high0, ret[0, c]) + dot(low0, ret[0, c])
+
     squares = jnp.zeros((tokens, 1), jnp.float32)
     for c in range(CHUNKS):
         shares[c].wait_recv()
@@ -245,8 +286,7 @@
         proxied[c].wait_send()
         shares[c].wait_send()
         for k in range(2):
-            await_bytes(send.at[k, c, pl.ds(cap, rows - cap)], d_send.at[k, c])
-            await_bytes(res.at[k, c, pl.ds(cap, rows - cap)], r_send.at[k, c])
+            await_bytes(send.at[k, c, pl.ds(cap, rows - cap)], r_send.at[k, c])
 
 
 def local(inputs, pre_gain, expert_ids, route_weights, gate_proj, up_proj, down_proj, post_gain):
@@ -287,11 +327,11 @@
             pltpu.VMEM((2, CHUNKS, rows, cw), bf16),
             pltpu.VMEM((2, CHUNKS, rows, cw), bf16),
             pltpu.VMEM((2, CHUNKS, rows, cw), bf16),
-            pltpu.VMEM((2, CHUNKS, rows, cw), bf16),
+            pltpu.VMEM((2, tps, rows, fh), jnp.float32),
             pltpu.VMEM((CHUNKS, tokens, cw), bf16),
             pltpu.VMEM((CHUNKS, tokens, cw), bf16),
             pltpu.VMEM((CHUNKS, tokens, cw), jnp.float32),
-            pltpu.VMEM((tps, rows, fh), bf16),
+            pltpu.VMEM((2, tps, rows, fh), bf16),
             pltpu.VMEM((2, 8, tokens), jnp.float32),
             dma((3,)), dma((3, tps - 1)), dma((3, tps - 1)),
             dma((CHUNKS,)), dma((CHUNKS,)), dma, dma,

time: 151 us -> 143 us (0.947)
  Pallas kernels: 147 us -> 139 us
    pallas_call x1, Pallas kernels: 147 us -> 139 us  [local(): pl.pallas_call(functools.partial(kernel, n, tps, cap), out_shape=jax.Shap...]
where the time goes in v2:
time: 143 us
  Pallas kernels  139 us (97%)
  local copies, waits for them, and re-layouts  2.38 us (2%)
  other arithmetic  2.03 us (1%)
    pallas_call x1, Pallas kernels, local(): pl.pallas_call(functools.partial(kernel, n, tps, cap), out_shape=jax.Shap...  139 us

profile of v2, /device:TPU:0, one launch (start us, length us, event | category | flops | bytes accessed | tf_op | source)
XLA Modules:
  0.0 143.0 jit_solution(14910470003516384915)
XLA Ops:
  0.0 0.1 pad.2.clone
  0.1 0.7 convert_element_type.3
  0.8 1.3 maximum_bitcast_fusion.meta_ref
  2.1 138.6 %shard_map.82 = bf16[256,2048]{1,0:T(8,128)(2,1)} custom-call(bf16[256,2048]{1,0:T(8,128)(2,1)} %x_ref.1, f32[1,2048]{1,0:T(1,128)} %bitcast.4, f32[8,256]{1,0:T(8,128)} %maximum_bitcast_fusion.meta_ref, bf16[1,2048,1024]{2,1,0:T(8,128)(2,1)} %gate_ref.1, bf16[1,2048,1024]{2,1,0:T(8,128)(2,1)} %up_ref.1, bf16[1,1024,2048]{2,1,0:T(8,128)(2,1)} %down_ref.1, ...), custom_call_target="tpu_custom_call" | custom-call | tf_op jit(solution)/shard_map/pallas_call | solution.py:315
  140.7 2.3 %copy.10 = bf16[256,2048]{1,0:T(8,128)(2,1)} copy(bf16[256,2048]{1,0:T(8,128)(2,1)} %shard_map.82) | data formatting | bytes 2097152
  (1 shorter events, 0.0 us)

commit v3 on v2

--- a/solution.py
+++ b/solution.py
@@ -173,7 +173,11 @@
     proxied[1].start()
     own(1)
     normalise(2)
+    proxied[2].start()
+    own(2)
     normalise(3)
+    proxied[3].start()
+    own(3)
     meta_copy.wait_recv()
     place(1, pmeta[...])
 
@@ -216,13 +220,11 @@
     both = range(tps)
     last = fh // TILE
     relay(0)
-    proxied[2].start()
     for copy in local_copies:
         copy.wait()
     for copy in peer_copies:
         copy.wait()
     relay(1)
-    proxied[3].start()
     received(1, 0)
     received(1, 1)
     expand(1, both, (0, 1), end=False)
@@ -230,8 +232,6 @@
     received(1, 2)
     expand(1, both, (2,), begin=False, end=False)
     relay(3)
-    own(2)
-    own(3)
     received(1, 3)
     expand(1, both, (3,), begin=False)
 

time: 143 us -> 144 us (level)
  no operation moved by 1% of the time
where the time goes in v3:
time: 144 us
  Pallas kernels  139 us (97%)
  local copies, waits for them, and re-layouts  2.38 us (2%)
  other arithmetic  2.03 us (1%)
    pallas_call x1, Pallas kernels, local(): pl.pallas_call(functools.partial(kernel, n, tps, cap), out_shape=jax.Shap...  139 us

profile of v3, /device:TPU:0, one launch (start us, length us, event | category | flops | bytes accessed | tf_op | source)
XLA Modules:
  0.0 143.6 jit_solution(16121268926493466465)
XLA Ops:
  0.0 0.1 pad.2.clone
  0.1 0.7 convert_element_type.3
  0.8 1.3 maximum_bitcast_fusion.meta_ref
  2.1 139.2 %shard_map.82 = bf16[256,2048]{1,0:T(8,128)(2,1)} custom-call(bf16[256,2048]{1,0:T(8,128)(2,1)} %x_ref.1, f32[1,2048]{1,0:T(1,128)} %bitcast.4, f32[8,256]{1,0:T(8,128)} %maximum_bitcast_fusion.meta_ref, bf16[1,2048,1024]{2,1,0:T(8,128)(2,1)} %gate_ref.1, bf16[1,2048,1024]{2,1,0:T(8,128)(2,1)} %up_ref.1, bf16[1,1024,2048]{2,1,0:T(8,128)(2,1)} %down_ref.1, ...), custom_call_target="tpu_custom_call" | custom-call | tf_op jit(solution)/shard_map/pallas_call | solution.py:315
  141.3 2.3 %copy.10 = bf16[256,2048]{1,0:T(8,128)(2,1)} copy(bf16[256,2048]{1,0:T(8,128)(2,1)} %shard_map.82) | data formatting | bytes 2097152
  (1 shorter events, 0.0 us)
